TPU v7x, 32 devices: a whole 2x2x4 slice. The times are simulated.
32 devices in a mesh: sp: 16 (over z, y, x), tp: 2 (over core).
Axes of the slice: x: 2, y: 2, z: 4, core: 2. Of those that a mesh axis runs over, the one named last changes fastest.
Arguments:
- query_one: bfloat16 [2048, 1024], P('sp', 'tp'), may hold values from -6 to 6
- key_one: bfloat16 [2048, 1024], P('sp', 'tp'), may hold values from -6 to 6
- query_two: bfloat16 [2048, 512], P('sp', 'tp'), may hold values from -6 to 6
- key_two: bfloat16 [2048, 512], P('sp', 'tp'), may hold values from -6 to 6
- values: bfloat16 [2048, 2048], P('sp', 'tp'), may hold values from -6 to 6
- out_gate: bfloat16 [2048, 2048], P('sp', 'tp'), may hold values from -6 to 6
- in_gate: float32 [16, 2048], P('tp', 'sp'), may hold values from -3 to 150
- forget_gate: float32 [16, 2048], P('tp', 'sp'), may hold values from -1 to 24
- head_gain: float32 [2048], P('tp'), may hold values from 0.1 to 1.9
- out_weight: bfloat16 [2048, 2048], P('tp'), may hold values from -0.125 to 0.125
- stream: bfloat16 [2048, 2048], P('sp'), may hold values from -6 to 6
- mix_gain: float32 [2048], replicated, may hold values from 0.1 to 1.9
- up_weight: bfloat16 [2048, 8192], P('sp', 'tp'), may hold values from -0.125 to 0.125
- down_weight: bfloat16 [8192, 2048], P('tp', 'sp'), may hold values from -0.0625 to 0.0625
- out_gain: float32 [2048], replicated, may hold values from 0.1 to 1.9
Outputs:
- result: bfloat16 [2048, 2048], P(('sp', 'tp'))
All inputs are finite; a program needn't handle non-finite values.
Results may differ from a plain program's by a relative error of at most 0.018.
Values may be sent and summed in bfloat16 or wider, within the bound.
A program may use at most 128 MiB of HBM per device.

v0:
```python
from functools import partial
import jax
import jax.numpy as jnp
from jax import lax
from jax.sharding import PartitionSpec as P

BLOCK = 64
NEG_BIG = -1e30
EPS = 1e-05


def prefix_2(part, axis, combine, identity):
    place = lax.axis_index(axis)
    gathered = jax.tree.map(lambda a: lax.all_gather(a, axis), part)
    state = jax.tree.map(lambda a, e: jnp.zeros_like(a) + jnp.asarray(e, a.dtype), part, identity)

    def one(lap, state):
        return combine(
            state, jax.tree.map(lambda a: lax.dynamic_index_in_dim(a, lap, 0, False), gathered)
        )

    return lax.fori_loop(0, place, one, state)


def combine(earlier, later):
    decay_early, cell_early, norm_early, peak_early = earlier
    decay_late, cell_late, norm_late, peak_late = later
    ceiling = jnp.maximum(decay_late + peak_early, peak_late)
    keep_share = jnp.exp(decay_late + peak_early - ceiling)
    fresh_share = jnp.exp(peak_late - ceiling)
    cell_new = keep_share[..., None, None] * cell_early + fresh_share[..., None, None] * cell_late
    norm_new = keep_share[..., None] * norm_early + fresh_share[..., None] * norm_late
    return (decay_early + decay_late, cell_new, norm_new, ceiling)


def combine_groups(earlier, later):
    return (combine(earlier[0], later[0]), combine(earlier[1], later[1]))


def summarize(queries, keys_in, values_in, in_pre, forget_pre, block_len):
    length, width_k = queries.shape
    block_count = length // block_len
    scaled_keys = keys_in.astype(jnp.float32).reshape(
        block_count, block_len, width_k
    ) * width_k ** (-0.5)
    values_f = values_in.astype(jnp.float32).reshape(block_count, block_len, -1)
    width_v = values_f.shape[-1]
    log_forget = jax.nn.log_sigmoid(forget_pre).reshape(block_count, block_len)
    log_input = in_pre.reshape(block_count, block_len)
    cumulative = jnp.cumsum(log_forget, 1)
    decay_total = cumulative[:, -1]
    weight_log = decay_total[:, None] - cumulative + log_input
    peak_log = jnp.max(weight_log, 1)
    weighted = jnp.exp(weight_log - peak_log[:, None])[..., None] * scaled_keys
    cell_states = jnp.einsum("cld,cle->cde", weighted, values_f, precision=lax.Precision.HIGHEST)
    norm_states = jnp.sum(weighted, 1)
    identity = (
        jnp.zeros((), jnp.float32),
        jnp.zeros((width_k, width_v), jnp.float32),
        jnp.zeros((width_k,), jnp.float32),
        jnp.full((), NEG_BIG, jnp.float32),
    )

    def advance(running, element):
        return (combine(running, element), running)

    closing, prefix = lax.scan(advance, identity, (decay_total, cell_states, norm_states, peak_log))
    return (closing, prefix, (scaled_keys, values_f, cumulative, log_input))


def finish(queries, prefix, pieces, incoming):
    scaled_keys, values_f, cumulative, log_input = pieces
    block_count, block_len, width_k = scaled_keys.shape
    spread_in = jax.tree.map(
        lambda leaf: jnp.broadcast_to(leaf, (block_count,) + leaf.shape), incoming
    )
    _, cell_states, norm_states, peaks = combine(spread_in, prefix)
    query_f = queries.astype(jnp.float32).reshape(block_count, block_len, width_k)
    log_gaps = cumulative[:, :, None] - cumulative[:, None, :] + log_input[:, None, :]
    causal = jnp.arange(block_len)[:, None] >= jnp.arange(block_len)[None, :]
    log_gaps = jnp.where(causal[None], log_gaps, -jnp.inf)
    carried = cumulative + peaks[:, None]
    ceiling = jnp.maximum(carried, jnp.max(log_gaps, 2))
    scores = jnp.einsum("cld,csd->cls", query_f, scaled_keys, precision=lax.Precision.HIGHEST)
    scores = scores * jnp.exp(log_gaps - ceiling[..., None])
    carry_weight = jnp.exp(carried - ceiling)
    numerator = carry_weight[..., None] * jnp.einsum(
        "cld,cde->cle", query_f, cell_states, precision=lax.Precision.HIGHEST
    )
    numerator = numerator + jnp.einsum(
        "cls,cse->cle", scores, values_f, precision=lax.Precision.HIGHEST
    )
    denominator = carry_weight * jnp.einsum(
        "cld,cd->cl", query_f, norm_states, precision=lax.Precision.HIGHEST
    )
    denominator = denominator + jnp.sum(scores, 2)
    result = numerator / jnp.maximum(jnp.abs(denominator), jnp.exp(-ceiling))[..., None]
    return result.reshape(block_count * block_len, -1)


def head_norm(cell_out):
    center = jnp.mean(cell_out, -1, keepdims=True)
    spread = jnp.mean(jnp.square(cell_out - center), -1, keepdims=True)
    return (cell_out - center) * lax.rsqrt(spread + EPS)


def layer_norm(rows_f, gain):
    center = jnp.mean(rows_f, -1, keepdims=True)
    spread = jnp.mean(jnp.square(rows_f - center), -1, keepdims=True)
    return (rows_f - center) * lax.rsqrt(spread + EPS) * gain


def empty_state(head_pairs, width_k, width_v):
    return (
        jnp.zeros((head_pairs,), jnp.float32),
        jnp.zeros((head_pairs, width_k, width_v), jnp.float32),
        jnp.zeros((head_pairs, width_k), jnp.float32),
        jnp.full((head_pairs,), NEG_BIG, jnp.float32),
    )


def body(
    query_one,
    key_one,
    query_two,
    key_two,
    values,
    out_gate,
    in_gate,
    forget_gate,
    head_gain,
    out_weight,
    stream,
    mix_gain,
    up_weight,
    down_weight,
    out_gain,
):
    length = stream.shape[0]
    head_pairs = in_gate.shape[0] // 2
    width_v = values.shape[1] // (2 * head_pairs)

    def split_heads(array):
        return array.reshape(length, head_pairs, -1).transpose(1, 0, 2)

    values_split = values.reshape(length, head_pairs, 2, width_v).transpose(1, 2, 0, 3)
    input_rows = in_gate.reshape(head_pairs, 2, length)
    forget_rows = forget_gate.reshape(head_pairs, 2, length)
    summary = jax.vmap(partial(summarize, block_len=BLOCK))
    queries_one = split_heads(query_one)
    queries_two = split_heads(query_two)
    closing_one, prefix_one, pieces_one = summary(
        queries_one, split_heads(key_one), values_split[:, 0], input_rows[:, 0], forget_rows[:, 0]
    )
    closing_two, prefix_two, pieces_two = summary(
        queries_two, split_heads(key_two), values_split[:, 1], input_rows[:, 1], forget_rows[:, 1]
    )
    identity = (
        empty_state(head_pairs, queries_one.shape[2], width_v),
        empty_state(head_pairs, queries_two.shape[2], width_v),
    )
    incoming = prefix_2((closing_one, closing_two), "sp", combine_groups, identity)
    cell_one = jax.vmap(finish)(queries_one, prefix_one, pieces_one, incoming[0])
    cell_two = jax.vmap(finish)(queries_two, prefix_two, pieces_two, incoming[1])
    normed = jnp.stack([head_norm(cell_one), head_norm(cell_two)], 1)
    normed = normed.transpose(2, 0, 1, 3).reshape(length, 2 * head_pairs * width_v)
    mixed_heads = (normed * head_gain * jax.nn.sigmoid(out_gate.astype(jnp.float32))).astype(
        jnp.bfloat16
    )
    own_rows = length // lax.axis_size("tp")
    leading = lax.axis_index("tp") * own_rows
    up_full, down_full = (
        lax.all_gather(up_weight, "sp", axis=0, tiled=True),
        lax.all_gather(down_weight, "sp", axis=1, tiled=True),
    )
    summed = lax.psum_scatter(
        jnp.dot(mixed_heads, out_weight, preferred_element_type=jnp.float32).astype(jnp.bfloat16),
        "tp",
        scatter_dimension=0,
        tiled=True,
    )
    mixer_out = lax.optimization_barrier(summed)
    stream_own = lax.dynamic_slice_in_dim(stream, leading, own_rows, 0)
    first_own = layer_norm(
        stream_own.astype(jnp.float32) + mixer_out.astype(jnp.float32), mix_gain
    ).astype(jnp.bfloat16)
    hidden = jnp.square(
        jax.nn.relu(
            jnp.dot(
                lax.all_gather(first_own, "tp", axis=0, tiled=True),
                up_full,
                preferred_element_type=jnp.float32,
            )
        )
    ).astype(jnp.bfloat16)
    partial_sums = jnp.dot(hidden, down_full, preferred_element_type=jnp.float32)
    mlp_out = lax.optimization_barrier(
        lax.psum_scatter(partial_sums.astype(jnp.bfloat16), "tp", scatter_dimension=0, tiled=True)
    )
    return layer_norm(first_own.astype(jnp.float32) + mlp_out.astype(jnp.float32), out_gain).astype(
        jnp.bfloat16
    )


def solution(mesh):
    in_specs = (
        P("sp", "tp"),
        P("sp", "tp"),
        P("sp", "tp"),
        P("sp", "tp"),
        P("sp", "tp"),
        P("sp", "tp"),
        P("tp", "sp"),
        P("tp", "sp"),
        P("tp"),
        P("tp", None),
        P("sp", None),
        P(),
        P("sp", "tp"),
        P("tp", "sp"),
        P(),
    )
    out_specs = P(("sp", "tp"), None)
    return jax.shard_map(body, mesh=mesh, in_specs=in_specs, out_specs=out_specs, check_vma=False)
```

profile of v0, /device:TPU:0, one launch (start us, length us, event | category | flops | bytes accessed | tf_op | source)
XLA Modules:
  0.0 683.7 jit_solution(4655088481596444945)
XLA Ops:
  6.6 0.8 fusion.72
  7.5 1.0 reduce_window_sum.18
  8.7 0.8 fusion.88
  9.8 1.1 reshape.275
  11.0 1.0 copy.76
  12.3 0.3 convolution_bitcast_fusion.3
  12.7 0.7 while.76
  13.4 0.6 copy-done.1
  14.2 1.0 reduce_window_sum.17
  16.2 0.7 convolution_bitcast_fusion
  16.9 0.8 while.75
  17.7 0.7 copy-done
  18.6 0.6 dynamic-slice
  19.7 0.2 dynamic-update-slice.2
  20.4 0.2 dynamic-update-slice.1
  20.6 43.8 %all-reduce.4 = (f32[64]{0:T(128)S(1)}, f32[64]{0:T(128)S(1)}, f32[64]{0:T(128)S(1)}, f32[64]{0:T(128)S(1)}) all-reduce(f32[64]{0:T(128)S(1)} %dynamic-update-slice, f32[64]{0:T(128)S(1)} %dynamic-update-slice.1, f32[64]{0:T(128)S(1)} %dynamic-update-slice.2, f32[64]{0:T(128)S(1)} %dynamic-update-slice.3), channel_id=2, replica_groups=mesh['sp'=16,'tp'=2] {'sp'}, use_global_device_ids=true, to_apply=%add | all-reduce | flops 256 | bytes 2048
  65.1 36.1 %all-gather.9 = f32[16,4,64]{2,1,0:T(4,128)S(1)} all-gather(f32[1,4,64]{2,1,0:T(4,128)S(1)} %bitcast.311), channel_id=9, replica_groups=mesh['sp'=16,'tp'=2] {'sp'}, dimensions={0}, use_global_device_ids=true | all-gather | bytes 17408 | tf_op jit(solution)/shard_map/all_gather | solution.py:14
  101.3 37.9 %all-gather.8 = f32[16,4,128]{2,1,0:T(4,128)S(1)} all-gather(f32[1,4,128]{2,1,0:T(4,128)S(1)} %bitcast.312), channel_id=5, replica_groups=mesh['sp'=16,'tp'=2] {'sp'}, dimensions={0}, use_global_device_ids=true | all-gather | bytes 34816 | tf_op jit(solution)/shard_map/all_gather | solution.py:14
  139.2 0.4 fusion.51
  139.6 15.4 %all-gather.19.cloned.1.call-done = f32[64,128,128]{2,1,0:T(8,128)} async-done(((f32[4,128,128]{2,1,0:T(8,128)}), f32[64,128,128]{2,1,0:T(8,128)}) %all-gather.19.cloned.1.call-update) | async-done | bytes 4194320 | tf_op jit(solution)/shard_map/all_gather | solution.py:14
  155.3 0.3 fusion.69
  155.7 0.4 fusion.91
  156.2 0.5 fusion.35
  156.7 0.5 fusion.92
  157.3 0.3 multiply_reduce_fusion.3
  157.7 0.2 fusion.60
  157.9 0.3 fusion.89
  158.4 0.4 fusion.32
  158.7 0.5 fusion.90
  159.3 0.3 multiply_reduce_fusion.2
  159.7 0.2 fusion.44
  160.2 0.4 copy.92
  160.6 0.4 reshape.286
  161.0 3.8 convolution_convert_fusion.1
  164.9 0.5 all-gather.15.cloned.1.call-update
  165.5 0.5 all-gather.17.cloned.1.call-update
  166.1 39.8 %reduce-scatter.3.cloned.1.call-done = bf16[64,2048]{1,0:T(8,128)(2,1)} async-done(((bf16[128,2048]{1,0:T(8,128)(2,1)}), bf16[64,2048]{1,0:T(8,128)(2,1)}) %reduce-scatter.3.cloned.1.call-update) | async-done | bytes 262160 | tf_op jit(solution)/shard_map/reduce_scatter | solution.py:176
  206.0 1.1 fusion.39
  207.1 1.2 multiply_reduce_fusion.1
  208.3 1.1 multiply_convert_fusion.1
  209.4 2.4 all_gather.73
  211.8 189.0 %all-gather.15.cloned.1.call-done = bf16[2048,4096]{1,0:T(8,128)(2,1)} async-done(((bf16[128,4096]{1,0:T(8,128)(2,1)}), bf16[2048,4096]{1,0:T(8,128)(2,1)}) %all-gather.15.cloned.1.call-update) | async-done | bytes 16777232 | tf_op jit(solution)/shard_map/all_gather | solution.py:173
  400.7 249.9 %all-gather.17.cloned.1.call-done = bf16[4096,2048]{1,0:T(8,128)(2,1)} async-done(((bf16[4096,128]{1,0:T(8,128)(2,1)}), bf16[4096,2048]{1,0:T(8,128)(2,1)}) %all-gather.17.cloned.1.call-update) | async-done | bytes 16777232 | tf_op jit(solution)/shard_map/all_gather | solution.py:174
  650.6 15.9 %convolution_convert_fusion = bf16[128,2048]{1,0:T(8,128)(2,1)} fusion(bf16[4096,2048]{1,0:T(8,128)(2,1)} %all-gather.17.cloned.1.call-done, bf16[128,2048]{1,0:T(8,128)(2,1)S(1)} %all_gather.73, bf16[2048,4096]{1,0:T(8,128)(2,1)} %all-gather.15.cloned.1.call-done), kind=kOutput, calls=%fused_computation.65 | convolution fusion | flops 4296802304 | bytes 34603008 | tf_op jit(solution)/shard_map/dot_general | solution.py:196
  666.5 6.3 reduce-scatter.5.cloned.1.call-done
  672.8 1.1 fusion.41
  673.9 1.2 multiply_reduce_fusion
  675.1 1.8 multiply_convert_fusion
  (157 shorter events, 6.3 us)
Async XLA Ops:
  6.5 9.0 %copy-start.3 = (bf16[128,512]{1,0:T(8,128)(2,1)S(1)}, bf16[128,512]{1,0:T(8,128)(2,1)}, u32[]{:S(2)}) copy-start(bf16[128,512]{1,0:T(8,128)(2,1)} %param.22) | copy-start | bytes 393220
  6.5 133.0 %all-gather.21.cloned.1.call-start = ((), (), s32[]{:S(2)}) async-start(), calls=%async_computation.7 | async-start | bytes 2228224 | tf_op jit(solution)/shard_map/all_gather | solution.py:14
  13.4 0.6 copy-start.1
  14.0 140.9 %all-gather.19.cloned.1.call-start = ((), (), s32[]{:S(2)}) async-start(), calls=%async_computation.6 | async-start | bytes 4456448 | tf_op jit(solution)/shard_map/all_gather | solution.py:14
  16.2 2.4 copy-start.10
  16.2 48.6 %copy-start.4 = (bf16[128,512]{1,0:T(8,128)(2,1)S(1)}, bf16[128,512]{1,0:T(8,128)(2,1)}, u32[]{:S(2)}) copy-start(bf16[128,512]{1,0:T(8,128)(2,1)} %param.21) | copy-start | bytes 393220
  16.9 48.0 %copy-start.5 = (bf16[128,256]{1,0:T(8,128)(2,1)S(1)}, bf16[128,256]{1,0:T(8,128)(2,1)}, u32[]{:S(2)}) copy-start(bf16[128,256]{1,0:T(8,128)(2,1)} %param.23) | copy-start | bytes 196612
  17.7 0.7 copy-start
  18.4 187.6 %reduce-scatter.3.cloned.1.call-start = ((), (), s32[]{:S(2)}) async-start(), calls=%async_computation.2 | async-start | bytes 786432 | tf_op jit(solution)/shard_map/reduce_scatter | solution.py:176
  157.2 3.8 copy-start.8
  157.2 3.8 copy-start.9
  161.0 44.9 %copy-start.2 = (bf16[128,2048]{1,0:T(8,128)(2,1)S(1)}, bf16[128,2048]{1,0:T(8,128)(2,1)}, u32[]{:S(2)}) copy-start(bf16[128,2048]{1,0:T(8,128)(2,1)} %param.31) | copy-start | bytes 1572868
  161.0 47.3 %copy-start.6 = (f32[2048]{0:T(1024)S(1)}, f32[2048]{0:T(1024)}, u32[]{:S(2)}) copy-start(f32[2048]{0:T(1024)} %param.32) | copy-start | bytes 24580
  164.9 235.8 %all-gather.15.cloned.1.call-start = ((), (), s32[]{:S(2)}) async-start(), calls=%async_computation.3 | async-start | bytes 17825792 | tf_op jit(solution)/shard_map/all_gather | solution.py:173
  165.5 485.1 %all-gather.17.cloned.1.call-start = ((), (), s32[]{:S(2)}) async-start(), calls=%async_computation.4 | async-start | bytes 17825792 | tf_op jit(solution)/shard_map/all_gather | solution.py:174
  166.1 506.7 %reduce-scatter.5.cloned.1.call-start = ((), (), s32[]{:S(2)}) async-start(), calls=%async_computation.5 | async-start | bytes 786432 | tf_op jit(solution)/shard_map/reduce_scatter | solution.py:198
  211.8 463.3 %copy-start.7 = (f32[2048]{0:T(1024)S(1)}, f32[2048]{0:T(1024)}, u32[]{:S(2)}) copy-start(f32[2048]{0:T(1024)} %param.35) | copy-start | bytes 24580
Sparse Core Ops, SparseCore 0:
  14.2 63.5 all-gather.20
  80.5 74.4 all-gather.18
  165.0 40.8 reduce-scatter.2
  208.6 192.1 all-gather.14
  403.3 247.2 all-gather.16
  666.6 6.0 reduce-scatter.4
where the time goes:
time: 685 us; the launch traced here: 684 us
  waiting for transfers between devices  501 us (73%)
  blocking collectives  120 us (18%)
  matrix products  23.7 us (3%)
  between operations  14.6 us (2%)
  other arithmetic  13.8 us (2%)
  local copies, waits for them, and re-layouts  9.5 us (1%)
    all_gather x1, waiting for transfers between devices, body(): lax.all_gather(down_weight, 'sp', axis=1, tiled=True)  250 us
    all_gather x1, waiting for transfers between devices, body(): lax.all_gather(up_weight, 'sp', axis=0, tiled=True)  189 us
    all_gather x2, blocking collectives, prefix_2(): gathered = jax.tree.map(lambda a: lax.all_gather(a, axis), part)  74.1 us
    unnamed x1, blocking collectives  43.8 us
    reduce_scatter x1, waiting for transfers between devices, body(): lax.psum_scatter(jnp.dot(mixed_heads, out_weight, preferred_element_type=...  39.8 us
    dot_general x1, matrix products, body(): jnp.dot(hidden, down_full, preferred_element_type=jnp.float32)  15.9 us
    all_gather x2, waiting for transfers between devices, prefix_2(): gathered = jax.tree.map(lambda a: lax.all_gather(a, axis), part)  15.4 us
  transfers between devices with their start and end apart: 6, of which 5 were waited for; matrix products, arithmetic and copies ran while one was open for 1% of the time, Pallas kernels for 0%

commit v1 on v0

--- a/solution.py
+++ b/solution.py
@@ -171,7 +171,7 @@
     leading = lax.axis_index("tp") * own_rows
     up_full, down_full = (
         lax.all_gather(up_weight, "sp", axis=0, tiled=True),
-        lax.all_gather(down_weight, "sp", axis=1, tiled=True),
+        jnp.concatenate(lax.all_gather(down_weight, "sp"), axis=1),
     )
     summed = lax.psum_scatter(
         jnp.dot(mixed_heads, out_weight, preferred_element_type=jnp.float32).astype(jnp.bfloat16),

time: 685 us -> 627 us (0.915)
  waiting for transfers between devices: 501 us -> 422 us
  local copies, waits for them, and re-layouts: 9.5 us -> 30.8 us
    all_gather x1, waiting for transfers between devices: 250 us -> 189 us  [body(): lax.all_gather(down_weight, 'sp')]
    reshape x0 -> x1, local copies, waits for them, and re-layouts: none -> 21.3 us  [body(): jnp.concatenate(lax.all_gather(down_weight, 'sp'), axis=1)]
    all_gather x1, waiting for transfers between devices: 189 us -> 171 us  [body(): lax.all_gather(up_weight, 'sp', axis=0, tiled=True)]
  transfers between devices with their start and end apart: 6 -> 6, of which waited for: 5 -> 5; matrix products, arithmetic and copies ran while one was open for 1% -> 5% of each run, Pallas kernels for 0% -> 0%
where the time goes in v1:
time: 627 us; the launch traced here: 625 us
  waiting for transfers between devices  422 us (67%)
  blocking collectives  120 us (19%)
  local copies, waits for them, and re-layouts  30.8 us (5%)
  matrix products  23.2 us (4%)
  between operations  14.7 us (2%)
  other arithmetic  13.8 us (2%)
    all_gather x1, waiting for transfers between devices, body(): lax.all_gather(down_weight, 'sp')  189 us
    all_gather x1, waiting for transfers between devices, body(): lax.all_gather(up_weight, 'sp', axis=0, tiled=True)  171 us
    all_gather x2, blocking collectives, prefix_2(): gathered = jax.tree.map(lambda a: lax.all_gather(a, axis), part)  74.1 us
    unnamed x1, blocking collectives  43.8 us
    reduce_scatter x1, waiting for transfers between devices, body(): lax.psum_scatter(jnp.dot(mixed_heads, out_weight, preferred_element_type=...  39.8 us
    reshape x1, local copies, waits for them, and re-layouts, body(): jnp.concatenate(lax.all_gather(down_weight, 'sp'), axis=1)  21.3 us
    dot_general x1, matrix products, body(): jnp.dot(hidden, down_full, preferred_element_type=jnp.float32)  15.4 us
    all_gather x2, waiting for transfers between devices, prefix_2(): gathered = jax.tree.map(lambda a: lax.all_gather(a, axis), part)  15.4 us
  transfers between devices with their start and end apart: 6, of which 5 were waited for; matrix products, arithmetic and copies ran while one was open for 5% of the time, Pallas kernels for 0%

profile of v1, /device:TPU:0, one launch (start us, length us, event | category | flops | bytes accessed | tf_op | source)
XLA Modules:
  0.0 625.2 jit_solution(11810433365940481148)
XLA Ops:
  6.6 0.8 fusion.72
  7.5 1.0 reduce_window_sum.18
  8.7 0.8 fusion.88
  9.8 1.1 reshape.281
  11.0 1.0 copy.103
  12.3 0.3 convolution_bitcast_fusion.3
  12.7 0.7 while.76
  13.4 0.6 copy-done.1
  14.2 1.0 reduce_window_sum.17
  16.2 0.7 convolution_bitcast_fusion
  16.9 0.8 while.75
  17.7 0.7 copy-done
  18.6 0.6 dynamic-slice
  19.7 0.2 dynamic-update-slice.2
  20.6 43.8 %all-reduce.4 = (f32[64]{0:T(128)S(1)}, f32[64]{0:T(128)S(1)}, f32[64]{0:T(128)S(1)}, f32[64]{0:T(128)S(1)}) all-reduce(f32[64]{0:T(128)S(1)} %dynamic-update-slice, f32[64]{0:T(128)S(1)} %dynamic-update-slice.1, f32[64]{0:T(128)S(1)} %dynamic-update-slice.2, f32[64]{0:T(128)S(1)} %dynamic-update-slice.3), channel_id=2, replica_groups=mesh['sp'=16,'tp'=2] {'sp'}, use_global_device_ids=true, to_apply=%add | all-reduce | flops 256 | bytes 2048
  65.1 36.1 %all-gather.10 = f32[16,4,64]{2,1,0:T(4,128)S(1)} all-gather(f32[1,4,64]{2,1,0:T(4,128)S(1)} %bitcast.317), channel_id=9, replica_groups=mesh['sp'=16,'tp'=2] {'sp'}, dimensions={0}, use_global_device_ids=true | all-gather | bytes 17408 | tf_op jit(solution)/shard_map/all_gather | solution.py:14
  101.3 37.9 %all-gather.9 = f32[16,4,128]{2,1,0:T(4,128)S(1)} all-gather(f32[1,4,128]{2,1,0:T(4,128)S(1)} %bitcast.318), channel_id=5, replica_groups=mesh['sp'=16,'tp'=2] {'sp'}, dimensions={0}, use_global_device_ids=true | all-gather | bytes 34816 | tf_op jit(solution)/shard_map/all_gather | solution.py:14
  139.2 0.4 fusion.51
  139.6 15.4 %all-gather.18.cloned.1.call-done = f32[64,128,128]{2,1,0:T(8,128)} async-done(((f32[4,128,128]{2,1,0:T(8,128)}), f32[64,128,128]{2,1,0:T(8,128)}) %all-gather.18.cloned.1.call-update) | async-done | bytes 4194320 | tf_op jit(solution)/shard_map/all_gather | solution.py:14
  155.3 0.3 fusion.69
  155.7 0.4 fusion.91
  156.2 0.5 fusion.35
  156.7 0.5 fusion.92
  157.3 0.3 multiply_reduce_fusion.3
  157.7 0.2 fusion.60
  157.9 0.3 fusion.89
  158.4 0.4 fusion.32
  158.7 0.5 fusion.90
  159.3 0.3 multiply_reduce_fusion.2
  159.7 0.2 fusion.44
  160.2 0.4 copy.119
  160.6 0.4 reshape.292
  161.0 3.8 convolution_convert_fusion.1
  164.9 0.5 all-gather.22.cloned.1.call-update
  165.5 0.5 all-gather.16.cloned.1.call-update
  166.1 39.8 %reduce-scatter.3.cloned.1.call-done = bf16[64,2048]{1,0:T(8,128)(2,1)} async-done(((bf16[128,2048]{1,0:T(8,128)(2,1)}), bf16[64,2048]{1,0:T(8,128)(2,1)}) %reduce-scatter.3.cloned.1.call-update) | async-done | bytes 262160 | tf_op jit(solution)/shard_map/reduce_scatter | solution.py:176
  206.0 1.1 fusion.39
  207.1 1.2 multiply_reduce_fusion.1
  208.3 1.1 multiply_convert_fusion.1
  209.4 2.4 all_gather.76
  211.8 189.0 %all-gather.22.cloned.1.call-done = bf16[65536,128]{1,0:T(8,128)(2,1)} async-done(((bf16[4096,128]{1,0:T(8,128)(2,1)}), bf16[65536,128]{1,0:T(8,128)(2,1)}) %all-gather.22.cloned.1.call-update) | async-done | bytes 16777232 | tf_op jit(solution)/shard_map/all_gather | solution.py:174
  400.7 21.3 %copy.120 = bf16[4096,16,128]{0,2,1:T(8,128)(2,1)} copy(bf16[4096,16,128]{2,0,1:T(8,128)(2,1)} %bitcast.300) | data formatting | bytes 33554432 | tf_op jit(solution)/shard_map/reshape | solution.py:174
  422.0 170.6 %all-gather.16.cloned.1.call-done = bf16[2048,4096]{1,0:T(8,128)(2,1)} async-done(((bf16[128,4096]{1,0:T(8,128)(2,1)}), bf16[2048,4096]{1,0:T(8,128)(2,1)}) %all-gather.16.cloned.1.call-update) | async-done | bytes 16777232 | tf_op jit(solution)/shard_map/all_gather | solution.py:173
  592.6 15.4 %convolution_convert_fusion = bf16[128,2048]{1,0:T(8,128)(2,1)} fusion(bf16[4096,2048]{0,1:T(8,128)(2,1)} %bitcast.299, bf16[128,2048]{1,0:T(8,128)(2,1)S(1)} %all_gather.76, bf16[2048,4096]{1,0:T(8,128)(2,1)} %all-gather.16.cloned.1.call-done), kind=kOutput, calls=%fused_computation.65 | convolution fusion | flops 4296802304 | bytes 34603008 | tf_op jit(solution)/shard_map/dot_general | solution.py:196
  608.0 6.3 %reduce-scatter.5.cloned.1.call-done = bf16[64,2048]{1,0:T(8,128)(2,1)} async-done(((bf16[128,2048]{1,0:T(8,128)(2,1)}), bf16[64,2048]{1,0:T(8,128)(2,1)}) %reduce-scatter.5.cloned.1.call-update) | async-done | bytes 262160 | tf_op jit(solution)/shard_map/reduce_scatter | solution.py:198
  614.3 1.1 fusion.41
  615.4 1.2 multiply_reduce_fusion
  616.6 1.8 multiply_convert_fusion
  (158 shorter events, 6.5 us)
Async XLA Ops:
  6.5 9.0 %copy-start.3 = (bf16[128,512]{1,0:T(8,128)(2,1)S(1)}, bf16[128,512]{1,0:T(8,128)(2,1)}, u32[]{:S(2)}) copy-start(bf16[128,512]{1,0:T(8,128)(2,1)} %param.22) | copy-start | bytes 393220
  6.5 133.0 %all-gather.20.cloned.1.call-start = ((), (), s32[]{:S(2)}) async-start(), calls=%async_computation.6 | async-start | bytes 2228224 | tf_op jit(solution)/shard_map/all_gather | solution.py:14
  13.4 0.6 copy-start.1
  14.0 140.9 %all-gather.18.cloned.1.call-start = ((), (), s32[]{:S(2)}) async-start(), calls=%async_computation.5 | async-start | bytes 4456448 | tf_op jit(solution)/shard_map/all_gather | solution.py:14
  16.2 2.4 copy-start.10
  16.2 48.6 %copy-start.4 = (bf16[128,512]{1,0:T(8,128)(2,1)S(1)}, bf16[128,512]{1,0:T(8,128)(2,1)}, u32[]{:S(2)}) copy-start(bf16[128,512]{1,0:T(8,128)(2,1)} %param.21) | copy-start | bytes 393220
  16.9 48.0 %copy-start.5 = (bf16[128,256]{1,0:T(8,128)(2,1)S(1)}, bf16[128,256]{1,0:T(8,128)(2,1)}, u32[]{:S(2)}) copy-start(bf16[128,256]{1,0:T(8,128)(2,1)} %param.23) | copy-start | bytes 196612
  17.7 0.7 copy-start
  18.4 187.6 %reduce-scatter.3.cloned.1.call-start = ((), (), s32[]{:S(2)}) async-start(), calls=%async_computation.2 | async-start | bytes 786432 | tf_op jit(solution)/shard_map/reduce_scatter | solution.py:176
  157.2 3.8 copy-start.8
  157.2 3.8 copy-start.9
  161.0 44.9 %copy-start.2 = (bf16[128,2048]{1,0:T(8,128)(2,1)S(1)}, bf16[128,2048]{1,0:T(8,128)(2,1)}, u32[]{:S(2)}) copy-start(bf16[128,2048]{1,0:T(8,128)(2,1)} %param.31) | copy-start | bytes 1572868
  161.0 47.3 %copy-start.6 = (f32[2048]{0:T(1024)S(1)}, f32[2048]{0:T(1024)}, u32[]{:S(2)}) copy-start(f32[2048]{0:T(1024)} %param.32) | copy-start | bytes 24580
  164.9 235.8 %all-gather.22.cloned.1.call-start = ((), (), s32[]{:S(2)}) async-start(), calls=%async_computation.7 | async-start | bytes 17825792 | tf_op jit(solution)/shard_map/all_gather | solution.py:174
  165.5 427.1 %all-gather.16.cloned.1.call-start = ((), (), s32[]{:S(2)}) async-start(), calls=%async_computation.3 | async-start | bytes 17825792 | tf_op jit(solution)/shard_map/all_gather | solution.py:173
  166.1 448.2 %reduce-scatter.5.cloned.1.call-start = ((), (), s32[]{:S(2)}) async-start(), calls=%async_computation.4 | async-start | bytes 786432 | tf_op jit(solution)/shard_map/reduce_scatter | solution.py:198
  592.6 24.0 %copy-start.7 = (f32[2048]{0:T(1024)S(1)}, f32[2048]{0:T(1024)}, u32[]{:S(2)}) copy-start(f32[2048]{0:T(1024)} %param.35) | copy-start | bytes 24580
Sparse Core Ops, SparseCore 0:
  14.2 63.5 all-gather.19
  80.5 74.4 all-gather.17
  165.0 40.8 reduce-scatter.2
  208.6 192.1 all-gather.21
  403.3 189.1 all-gather.15
  608.1 6.0 reduce-scatter.4
